TPU v7x, 32 devices: a whole 2x2x4 slice. The times are simulated.
32 devices in a mesh: grp: 2 (over y), ep: 8 (over z, x), tp: 2 (over core).
Axes of the slice: x: 2, y: 2, z: 4, core: 2. Of those that a mesh axis runs over, the one named last changes fastest.
Arguments:
- tokens: bfloat16 [4096, 2048], P(('grp', 'ep', 'tp')), parts along dimension 0, may hold values from -6 to 6
- expert_ids: int32 [4096, 4], P(('grp', 'ep', 'tp')), parts along dimension 0, may hold values from 0 to 15, all different within a row; in each aligned block of 128 rows (0 to 127, 128 to 255, ...) at most 48 rows name the same one
- gate_weights: float32 [4096, 4], P(('grp', 'ep', 'tp')), parts along dimension 0, may hold values from 0.1 to 1
- norm_gain: float32 [2048], replicated, may hold values from 0.1 to 1.9
- expert_gate: bfloat16 [16, 2048, 512], P(('ep', 'tp')), may hold values from -0.125 to 0.125
- expert_up: bfloat16 [16, 2048, 512], P(('ep', 'tp')), may hold values from -0.125 to 0.125
- expert_down: bfloat16 [16, 512, 2048], P(('ep', 'tp'))
- shared_gate: bfloat16 [2048, 512], P(None, 'tp'), may hold values from -0.125 to 0.125
- shared_up: bfloat16 [2048, 512], P(None, 'tp'), may hold values from -0.125 to 0.125
- shared_down: bfloat16 [512, 2048], P('tp')
- out_gain: float32 [2048], replicated, may hold values from 0.1 to 1.9
Outputs:
- layer_out: bfloat16 [4096, 2048], P(('grp', 'ep'), 'tp'), parts along dimension 0
There are 2 independent parts, one for each index of `grp`. A program takes and returns all parts, laid end to end along the dimension named above; an argument that names none is the same for every part. Nothing has to cross between parts.
Inputs may be any that keep to these rules, and one draw needn't show every extreme that they name: `expert_ids`: each row names 4 different experts. Among the 128 rows of one device (aligned blocks of rows), no expert is named more than 48 times, and in every draw some expert is named exactly 48 times by some device.
All inputs are finite; a program needn't handle non-finite values.
Results may differ from a plain program's by a relative error of at most 0.0085.
Values may be sent and summed in bfloat16 or wider, within the bound.
A program may use at most 64 MiB of HBM per device.

v0:
```python
import jax
import jax.numpy as jnp
from jax import lax
from jax.sharding import PartitionSpec as P

TOPK = 4


def expert_work(received, expert_gate, expert_up, expert_down):
    gate = jnp.einsum("slcd,ldf->slcf", received, expert_gate, preferred_element_type=jnp.float32)
    upper = jnp.einsum("slcd,ldf->slcf", received, expert_up, preferred_element_type=jnp.float32)
    hidden = (jax.nn.silu(gate) * upper).astype(jnp.bfloat16)
    return jnp.einsum(
        "slcf,lfd->slcd", hidden, expert_down, preferred_element_type=jnp.float32
    ).astype(jnp.bfloat16)


def local(
    tokens,
    expert_ids,
    gate_weights,
    norm_gain,
    expert_gate,
    expert_up,
    expert_down,
    shared_gate,
    shared_up,
    shared_down,
    out_gain,
):
    local_rows = tokens.shape[0]
    width = tokens.shape[1]
    ep_count = lax.axis_size("ep")
    tp_count = lax.axis_size("tp")
    device_count = ep_count * tp_count
    local_experts = expert_gate.shape[0]
    expert_count = device_count * local_experts
    capacity = 3 * local_rows * TOPK // (2 * expert_count)
    values = tokens.astype(jnp.float32)
    scale = lax.rsqrt(jnp.mean(values * values, axis=1, keepdims=True) + 1e-06)
    normed = (values * scale * norm_gain).astype(jnp.bfloat16)
    flat_ids = expert_ids.reshape(-1)
    one_hot = (flat_ids[:, None] == jnp.arange(expert_count, dtype=jnp.int32)[None, :]).astype(
        jnp.int32
    )
    earlier = jnp.cumsum(one_hot, axis=0) - one_hot
    slot_index = jnp.sum(earlier * one_hot, axis=1)
    target = flat_ids * capacity + slot_index
    copy_rows = normed[jnp.arange(local_rows * TOPK, dtype=jnp.int32) // TOPK]
    outgoing = jnp.zeros((expert_count * capacity, width), jnp.bfloat16).at[target].set(copy_rows)
    sending = outgoing.reshape(device_count, local_experts * capacity, width)
    received = lax.all_to_all(sending, ("ep", "tp"), split_axis=0, concat_axis=0, tiled=True)
    received = received.reshape(device_count, local_experts, capacity, width)
    results = expert_work(received, expert_gate, expert_up, expert_down)
    results = results.reshape(device_count, local_experts * capacity, width)
    returned = lax.all_to_all(results, ("ep", "tp"), split_axis=0, concat_axis=0, tiled=True)
    returned = returned.reshape(expert_count * capacity, width)
    picked = returned[target].astype(jnp.float32).reshape(local_rows, TOPK, width)
    routed = jnp.sum(picked * gate_weights[:, :, None], axis=1)
    piece = lax.all_gather(normed, "tp", axis=0, tiled=True)
    gate = jnp.dot(piece, shared_gate, preferred_element_type=jnp.float32)
    upper = jnp.dot(piece, shared_up, preferred_element_type=jnp.float32)
    shared_hidden = (jax.nn.silu(gate) * upper).astype(jnp.bfloat16)
    shared_out = lax.psum_scatter(
        jnp.dot(shared_hidden, shared_down, preferred_element_type=jnp.float32),
        "tp",
        scatter_dimension=0,
        tiled=True,
    )
    mixed = (routed + shared_out).astype(jnp.bfloat16)
    mixed_values = mixed.astype(jnp.float32)
    final_scale = lax.rsqrt(jnp.mean(mixed_values * mixed_values, axis=1, keepdims=True) + 1e-06)
    normalized = (mixed_values * final_scale * out_gain).astype(jnp.bfloat16)
    return lax.all_to_all(normalized, "tp", split_axis=1, concat_axis=0, tiled=True)


def solution(mesh):
    in_specs = (
        P(("grp", "ep", "tp"), None),
        P(("grp", "ep", "tp"), None),
        P(("grp", "ep", "tp"), None),
        P(),
        P(("ep", "tp"), None, None),
        P(("ep", "tp"), None, None),
        P(("ep", "tp"), None, None),
        P(None, "tp"),
        P(None, "tp"),
        P("tp", None),
        P(),
    )
    out_specs = P(("grp", "ep"), "tp")
    return jax.shard_map(local, mesh=mesh, in_specs=in_specs, out_specs=out_specs, check_vma=False)
```

profile of v0, /device:TPU:21, one launch (start us, length us, event | category | flops | bytes accessed | tf_op | source)
XLA Modules:
  0.0 220.6 jit_solution(6579901124432429304)
XLA Ops:
  6.5 0.0 copy-start
  6.5 0.9 copy.21
  7.5 0.1 eq.29
  7.6 0.1 eq.25
  7.7 0.7 broadcast_multiply_fusion
  8.4 1.2 reduce-window.6
  9.6 0.2 slice_reduce_fusion
  9.8 0.1 copy.20
  9.9 0.1 mul.81
  10.0 1.2 fusion.19
  11.3 0.1 fusion.35
  11.4 1.2 fusion.21
  12.6 0.0 copy-start.3
  12.6 12.3 %scatter_custom_fusion = bf16[768,2048]{1,0:T(8,128)(2,1)} fusion(s32[512]{0:T(512)S(1)} %bitcast.97, bf16[128,2048]{1,0:T(8,128)(2,1)S(1)} %fusion.21, s32[1024]{0:T(1024)S(1)} %pad_clamp_fusion.1, bf16[]{:T(256)} %constant.32.clone.1), kind=kCustom, calls=%fused_computation.10 | custom fusion | bytes 3145730 | tf_op jit(solution)/shard_map/scatter | solution.py:50
  25.0 0.0 copy-start.6
  25.0 75.9 %all_to_all.29 = bf16[16,48,2048]{2,1,0:T(8,128)(2,1)S(1)} all-to-all(bf16[16,48,2048]{2,1,0:T(8,128)(2,1)} %bitcast.93), channel_id=1, replica_groups=mesh['grp'=2,'ep'=8,'tp'=2] {'ep','tp'}, dimensions={0} | all-to-all | bytes 6291456 | tf_op jit(solution)/shard_map/all_to_all | solution.py:52
  100.8 0.0 copy-done.3
  100.8 0.0 copy-start.2
  100.8 1.7 copy-done.2
  102.5 0.0 copy-done.6
  102.5 2.9 %fusion.3 = f32[16,48,512]{2,1,0:T(8,128)} fusion(bf16[16,48,2048]{2,1,0:T(8,128)(2,1)S(1)} %all_to_all.29, bf16[1,2048,512]{2,1,0:T(8,128)(2,1)S(1)} %copy-done.6), kind=kOutput, calls=%fused_computation.8 | convolution fusion | flops 1610612736 | bytes 6815744 | tf_op jit(solution)/shard_map/slcd,ldf->slcf/dot_general | solution.py:10
  105.4 0.0 copy-done
  105.4 8.1 %convolution_convert_fusion = bf16[16,48,2048]{2,1,0:T(8,128)(2,1)} fusion(bf16[1,512,2048]{2,1,0:T(8,128)(2,1)S(1)} %copy-done, bf16[16,48,2048]{2,1,0:T(8,128)(2,1)} %copy-done.2, bf16[1,2048,512]{2,1,0:T(8,128)(2,1)} %param.16, f32[16,48,512]{2,1,0:T(8,128)} %fusion.3), kind=kOutput, calls=%fused_computation.4 | convolution fusion | flops 3225157632 | bytes 12058624 | tf_op jit(solution)/shard_map/slcf,lfd->slcd/dot_general | solution.py:13
  113.6 5.6 %all-to-all-start.1 = ((bf16[16,48,2048]{2,1,0:T(8,128)(2,1)}), bf16[16,48,2048]{2,1,0:T(8,128)(2,1)}, u32[]{:S(2)}, u32[]{:S(2)}) async-start(bf16[16,48,2048]{2,1,0:T(8,128)(2,1)} %convolution_convert_fusion), calls=%async_computation.1 | async-start | bytes 6291456 | tf_op jit(solution)/shard_map/all_to_all | solution.py:56
  119.2 0.0 all-gather.2.cloned.1.call-start
  119.2 0.7 all-gather.2.cloned.1.call-update
  119.9 0.0 reduce-scatter.2.cloned.1.call-start
  119.9 12.0 %all-gather.2.cloned.1.call-done = bf16[256,2048]{1,0:T(8,128)(2,1)} async-done(((bf16[128,2048]{1,0:T(8,128)(2,1)}), bf16[256,2048]{1,0:T(8,128)(2,1)}) %all-gather.2.cloned.1.call-update) | async-done | bytes 1048592 | tf_op jit(solution)/shard_map/all_gather | solution.py:60
  131.9 0.0 copy-start.1
  131.9 2.1 fusion.39
  134.0 0.0 copy-done.1
  134.0 4.2 %fusion.18 = f32[256,2048]{1,0:T(8,128)} fusion(bf16[256,2048]{1,0:T(8,128)(2,1)} %param.20, bf16[256,2048]{1,0:T(8,128)(2,1)S(1)} %copy-done.1, bf16[2048,256]{1,0:T(8,128)(2,1)} %param.19, f32[256,256]{1,0:T(8,128)S(1)} %fusion.39), kind=kOutput, calls=%fused_computation.27 | convolution fusion | flops 537264128 | bytes 5505024 | tf_op jit(solution)/shard_map/dot_general | solution.py:65
  138.2 0.0 copy-start.5
  138.2 0.0 reduce-scatter.2.cloned.1.call-update
  138.2 0.7 copy-done.5
  138.9 0.1 copy.24
  139.0 49.8 %all-to-all-done.1 = bf16[16,48,2048]{2,1,0:T(8,128)(2,1)} async-done(((bf16[16,48,2048]{2,1,0:T(8,128)(2,1)}), bf16[16,48,2048]{2,1,0:T(8,128)(2,1)}, u32[]{:S(2)}, u32[]{:S(2)}) %all-to-all-start.1) | async-done | bytes 3145760 | tf_op jit(solution)/shard_map/all_to_all | solution.py:56
  188.8 7.6 %gather_fusion = bf16[512,2048]{1,0:T(8,128)(2,1)} fusion(bf16[768,2048]{1,0:T(8,128)(2,1)} %bitcast.20, s32[1024]{0:T(1024)S(1)} %pad_clamp_fusion), kind=kCustom, calls=%fused_computation.1 | custom fusion | bytes 4196352 | tf_op jit(solution)/shard_map/gather | solution.py:58
  196.3 4.8 %reshape.150 = f32[128,4,2048]{2,1,0:T(4,128)} reshape(bf16[512,2048]{1,0:T(8,128)(2,1)} %gather_fusion) | data formatting | bytes 6291456 | tf_op jit(solution)/shard_map/convert_element_type | solution.py:58
  201.1 5.4 %multiply_reduce_fusion = f32[128,2048]{1,0:T(8,128)S(1)} fusion(f32[128,4,2048]{2,1,0:T(4,128)} %reshape.150, f32[128,4]{1,0:T(8,128)S(1)} %copy.24), kind=kLoop, calls=%fused_computation.3 | loop fusion | flops 1835008 | bytes 5244928 | tf_op jit(solution)/shard_map/reduce_sum | solution.py:59
  206.5 0.0 copy-start.4
  206.5 0.0 reduce-scatter.2.cloned.1.call-done
  206.5 1.4 fusion.22
  208.0 0.0 copy-done.4
  208.0 0.2 fusion.24
  208.2 4.8 %all_to_all.30 = bf16[128,2,1024]{2,0,1:T(8,128)(2,1)S(1)} all-to-all(bf16[128,2,1024]{2,0,1:T(8,128)(2,1)S(1)} %bitcast.95), channel_id=1, replica_groups=mesh['grp'=2,'ep'=8,'tp'=2] {'tp'}, dimensions={1} | all-to-all | bytes 1048576 | tf_op jit(solution)/shard_map/all_to_all | solution.py:74
  213.0 0.8 copy.32
  (10 shorter events, 0.1 us)
Async XLA Ops:
  6.5 98.9 %copy-start = (bf16[1,512,2048]{2,1,0:T(8,128)(2,1)S(1)}, bf16[1,512,2048]{2,1,0:T(8,128)(2,1)}, u32[]{:S(2)}) copy-start(bf16[1,512,2048]{2,1,0:T(8,128)(2,1)} %param.17) | copy-start | bytes 6291460
  12.6 88.2 %copy-start.3 = (bf16[128,2048]{1,0:T(8,128)(2,1)}, bf16[128,2048]{1,0:T(8,128)(2,1)S(1)}, u32[]{:S(2)}) copy-start(bf16[128,2048]{1,0:T(8,128)(2,1)S(1)} %fusion.21) | copy-start | bytes 1572868
  25.0 77.6 %copy-start.6 = (bf16[1,2048,512]{2,1,0:T(8,128)(2,1)S(1)}, bf16[1,2048,512]{2,1,0:T(8,128)(2,1)}, u32[]{:S(2)}) copy-start(bf16[1,2048,512]{2,1,0:T(8,128)(2,1)} %param.15) | copy-start | bytes 6291460
  100.8 1.7 copy-start.2
  113.6 75.2 %all-to-all-start.1 = ((bf16[16,48,2048]{2,1,0:T(8,128)(2,1)}), bf16[16,48,2048]{2,1,0:T(8,128)(2,1)}, u32[]{:S(2)}, u32[]{:S(2)}) async-start(bf16[16,48,2048]{2,1,0:T(8,128)(2,1)} %convolution_convert_fusion), calls=%async_computation.1 | async-start | bytes 6291456 | tf_op jit(solution)/shard_map/all_to_all | solution.py:56
  119.2 12.7 %all-gather.2.cloned.1.call-start = ((), (), s32[]{:S(2)}) async-start(), calls=%async_computation.4 | async-start | bytes 1572864 | tf_op jit(solution)/shard_map/all_gather | solution.py:60
  119.9 86.6 %reduce-scatter.2.cloned.1.call-start = ((), (), s32[]{:S(2)}) async-start(), calls=%async_computation.5 | async-start | bytes 3145728 | tf_op jit(solution)/shard_map/reduce_scatter | solution.py:64
  131.9 2.1 copy-start.1
  138.2 0.7 copy-start.5
  206.5 1.5 copy-start.4
Sparse Core Ops, SparseCore 0:
  121.5 10.3 all-gather.1
  138.3 10.8 reduce-scatter.1
where the time goes:
time: 221 us
  blocking collectives  80.6 us (36%)
  waiting for transfers between devices  62.5 us (28%)
  local copies, waits for them, and re-layouts  29.6 us (13%)
  matrix products  17.3 us (8%)
  between operations  13.5 us (6%)
  other arithmetic  11.5 us (5%)
  starting transfers between devices  5.64 us (3%)
    all_to_all x1, blocking collectives, local(): lax.all_to_all(sending, ('ep', 'tp'), split_axis=0, concat_axis=0, tiled=...  75.9 us
    all_to_all x1, waiting for transfers between devices, local(): lax.all_to_all(results, ('ep', 'tp'), split_axis=0, concat_axis=0, tiled=...  49.8 us
    scatter x1, local copies, waits for them, and re-layouts, local(): jnp.zeros((expert_count * capacity, width), jnp.bfloat16).at[target]  12.3 us
    all_gather x1, waiting for transfers between devices, local(): piece = lax.all_gather(normed, 'tp', axis=0, tiled=True)  12 us
    dot_general x1, matrix products, expert_work(): jnp.einsum('slcf,lfd->slcd', hidden, expert_down, preferred_element_type=...  8.14 us
    gather x1, local copies, waits for them, and re-layouts, local(): returned[target].astype(jnp.float32).reshape(local_rows, TOPK, width)  7.58 us
    all_to_all x1, starting transfers between devices, local(): lax.all_to_all(results, ('ep', 'tp'), split_axis=0, concat_axis=0, tiled=...  5.56 us
    reduce_sum x1, other arithmetic, local(): routed = jnp.sum(picked * gate_weights[:, :, None], axis=1)  5.35 us
  transfers between devices with their start and end apart: 3, of which 2 were waited for; matrix products, arithmetic and copies ran while one was open for 11% of the time, Pallas kernels for 0%

commit v1 on v0

--- a/solution.py
+++ b/solution.py
@@ -1,7 +1,393 @@
+import functools
+
 import jax
 import jax.numpy as jnp
 from jax import lax
+from jax.experimental import pallas as pl
+from jax.experimental.pallas import tpu as pltpu
 from jax.sharding import PartitionSpec as P
+
+MESH = pl.DeviceIdType.MESH
+F32 = jnp.float32
+BF16 = jnp.bfloat16
+
+
+def ring_kernel(
+    n,
+    ids_ref,
+    gates_ref,
+    tok_ref,
+    gain_ref,
+    out_gain_ref,
+    eg_hbm,
+    eu_hbm,
+    ed_hbm,
+    sg_hbm,
+    su_hbm,
+    sd_hbm,
+    out_ref,
+    own_x,
+    own_w,
+    rx,
+    wrx,
+    wg,
+    wu,
+    wd_mine,
+    wd_other,
+    sg,
+    su,
+    sd_mine,
+    sd_other,
+    kept,
+    psend,
+    prx,
+    home,
+    home_send,
+    home_rx,
+    rs_send,
+    rs_rx,
+    sq_send,
+    sq_rx,
+    load_sem,
+    ag_ssem,
+    ag_rsem,
+    w_ssem,
+    w_rsem,
+    pag_ssem,
+    pag_rsem,
+    pw_ssem,
+    pw_rsem,
+    ox_ssem,
+    ox_rsem,
+    p_ssem,
+    p_rsem,
+    h_ssem,
+    h_rsem,
+    rs_ssem,
+    rs_rsem,
+    sq_ssem,
+    sq_rsem,
+):
+    slots = n - 1
+    rows, width = tok_ref.shape
+    half = rows // 2
+    cols = width // 2
+    topk = ids_ref.shape[1]
+    experts = own_w.shape[1]
+    turn = n // 2
+    ep = lax.axis_index("ep")
+    c = lax.axis_index("tp")
+    oc = 1 - c
+    x = ep % 2
+    z = ep // 2
+    pos = z * (1 - x) + (n - 1 - z) * x
+
+    def at(p):
+        q = p // turn
+        return 2 * p * (1 - q) + (2 * (n - 1 - p) + 1) * q
+
+    toward = (at((pos + 1) % n), at((pos + n - 1) % n))
+    mine = ep * 2 + c
+
+    barrier = pltpu.get_barrier_semaphore()
+    for e in toward:
+        pl.semaphore_signal(barrier, inc=1, device_id={"ep": e, "tp": c}, device_id_type=MESH)
+    pl.semaphore_signal(barrier, inc=1, device_id={"ep": ep, "tp": oc}, device_id_type=MESH)
+
+    lo, hi = pl.ds(pl.multiple_of(c * cols, cols), cols), pl.ds(pl.multiple_of(oc * cols, cols), cols)
+    loads = [
+        (eg_hbm.at[0], wg),
+        (eu_hbm.at[0], wu),
+        (ed_hbm.at[0, :, hi], wd_other),
+        (ed_hbm.at[0, :, lo], wd_mine),
+        (sg_hbm, sg),
+        (su_hbm, su),
+        (sd_hbm.at[:, hi], sd_other),
+        (sd_hbm.at[:, lo], sd_mine),
+    ]
+    loads = [pltpu.make_async_copy(s, d, load_sem.at[i]) for i, (s, d) in enumerate(loads)]
+    for load in loads:
+        load.start()
+
+    values = tok_ref[...].astype(F32)
+    scale = lax.rsqrt(jnp.mean(values * values, axis=1, keepdims=True) + 1e-06)
+    own_x[c] = (values * scale * gain_ref[...]).astype(BF16)
+    lane = lax.broadcasted_iota(jnp.int32, (rows, 128), 1)
+    dense = jnp.zeros((rows, 128), F32)
+    for k in range(topk):
+        dense += jnp.where(ids_ref[:, k : k + 1] == lane, gates_ref[:, k : k + 1], 0.0)
+    own_w[c] = dense.T[:experts]
+
+    pl.semaphore_wait(barrier, 3)
+
+    def remote(src, dst, ssem, rsem, e, core):
+        return pltpu.make_async_remote_copy(
+            src_ref=src,
+            dst_ref=dst,
+            send_sem=ssem,
+            recv_sem=rsem,
+            device_id={"ep": e, "tp": core},
+            device_id_type=MESH,
+        )
+
+    def ag(s, d, src):
+        return remote(src, rx.at[s, d, c], ag_ssem.at[s, d], ag_rsem.at[s, d], toward[d], c)
+
+    def agw(i, d, src):
+        return remote(src, wrx.at[i, d, c], w_ssem.at[i, d], w_rsem.at[i, d], toward[d], c)
+
+    def pag(s, d, core):
+        return remote(
+            rx.at[s, d, core], rx.at[s, d, core], pag_ssem.at[s, d], pag_rsem.at[s, d], ep, oc
+        )
+
+    def pagw(i, d, core):
+        return remote(
+            wrx.at[i, d, core], wrx.at[i, d, core], pw_ssem.at[i, d], pw_rsem.at[i, d], ep, oc
+        )
+
+    def own_half(h):
+        return own_x.at[c, pl.ds(h * half, half)]
+
+    for d in range(2):
+        agw(0, d, own_w.at[c]).start()
+        ag(0, d, own_half(d)).start()
+    home_copies = (
+        lambda core: remote(own_x.at[core], own_x.at[core], ox_ssem.at[0], ox_rsem.at[0], ep, oc),
+        lambda core: remote(own_w.at[core], own_w.at[core], ox_ssem.at[1], ox_rsem.at[1], ep, oc),
+    )
+    for copy in home_copies:
+        copy(c).start()
+    for d in range(2):
+        ag(1, d, own_half(1 - d)).start()
+
+    def silu_mul(g, u):
+        return (g / (1.0 + jnp.exp(-g)) * u).astype(BF16)
+
+    def dot(a, b):
+        return jnp.dot(a, b, preferred_element_type=F32)
+
+    def column(row, offset, count):
+        r = lax.broadcasted_iota(jnp.int32, (count, rows), 0) + offset
+        q = lax.broadcasted_iota(jnp.int32, (count, rows), 1)
+        return jnp.sum(jnp.where(r == q, row, 0.0), axis=1, keepdims=True)
+
+    for load in loads:
+        load.wait()
+    for copy in home_copies:
+        copy(oc).wait_recv()
+
+    xs = own_x[...].reshape(2 * rows, width)
+    hidden = silu_mul(dot(xs, wg[...]), dot(xs, wu[...]))
+    shared = silu_mul(dot(xs, sg[...]), dot(xs, su[...]))
+    weight = jnp.concatenate(
+        [column(own_w[k, pl.ds(mine, 1), :], 0, rows) for k in range(2)], axis=0
+    )
+    home_send[...] = dot(hidden, wd_other[...]) * weight + dot(shared, sd_other[...])
+    home[...] = dot(hidden, wd_mine[...]) * weight + dot(shared, sd_mine[...])
+    home_copy = remote(home_send, home_rx, h_ssem.at[0], h_rsem.at[0], ep, oc)
+    home_copy.start()
+
+    def partner(s):
+        return remote(psend.at[s], prx.at[s], p_ssem.at[s], p_rsem.at[s], ep, oc)
+
+    def step(s, _):
+        i = s // 2
+        even = s % 2 == 0
+        for d in range(2):
+            ag(s, d, rx.at[s, d, c]).wait_recv()
+
+            @pl.when(s + 2 < slots)
+            def _():
+                ag(s + 2, d, rx.at[s, d, c]).start()
+
+            pag(s, d, c).start()
+
+            @pl.when(even)
+            def _():
+                agw(i, d, wrx.at[i, d, c]).wait_recv()
+
+                @pl.when(s + 2 < slots)
+                def _():
+                    agw(i + 1, d, wrx.at[i, d, c]).start()
+
+                pagw(i, d, c).start()
+
+        for d in range(2):
+            pag(s, d, oc).wait_recv()
+
+            @pl.when(even)
+            def _():
+                pagw(i, d, oc).wait_recv()
+
+        weight = jnp.concatenate(
+            [
+                column(
+                    wrx[i, d, k, pl.ds(mine, 1), :],
+                    (s % 2) * half if d == 0 else (1 - s % 2) * half,
+                    half,
+                )
+                for d in range(2)
+                for k in range(2)
+            ],
+            axis=0,
+        )
+        xs = rx[s].reshape(2 * rows, width)
+        hidden = silu_mul(dot(xs, wg[...]), dot(xs, wu[...]))
+        psend[s] = (dot(hidden, wd_other[...]) * weight).astype(BF16)
+        kept[s] = dot(hidden, wd_mine[...]) * weight
+        partner(s).start()
+        return 0
+
+    def back(s, d):
+        return remote(
+            rs_send.at[s, d], rs_rx.at[s, d], rs_ssem.at[s, d], rs_rsem.at[s, d], toward[1 - d], c
+        )
+
+    def give(s, further):
+        partner(s).wait_recv()
+        for d in range(2):
+            part = pl.ds(d * rows, rows)
+            total = kept[s, part, :] + prx[s, part, :].astype(F32)
+            if further:
+                back(s + 2, d).wait_recv()
+                total += rs_rx[s + 2, d].astype(F32)
+            rs_send[s, d] = total.astype(BF16)
+            back(s, d).start()
+
+    lax.fori_loop(0, slots - 1, step, 0)
+    give(slots - 2, False)
+    lax.fori_loop(slots - 1, slots, step, 0)
+    give(slots - 1, False)
+    for s in [t for k in range(slots - 4, -1, -2) for t in (k, k + 1)] + [0]:
+        give(s, True)
+
+    home_copy.wait_recv()
+    mixed = []
+    for s in range(2):
+        for d in range(2):
+            back(s, d).wait_recv()
+    for k in range(2):
+        for h in range(2):
+            part = pl.ds(k * rows + h * half, half)
+            got = pl.ds(k * half, half)
+            total = home[part, :] + home_rx[part, :]
+            total += rs_rx[h, 0, got, :].astype(F32) + rs_rx[1 - h, 1, got, :].astype(F32)
+            rounded = total.astype(BF16).astype(F32)
+            home[part, :] = rounded
+            sq = jnp.sum(rounded * rounded, axis=1, keepdims=True)
+            sq_send[part, :] = jnp.broadcast_to(sq, (half, 128))
+    sq_copy = remote(sq_send, sq_rx, sq_ssem.at[0], sq_rsem.at[0], ep, oc)
+    sq_copy.start()
+    sq_copy.wait_recv()
+    total = (sq_send[...] + sq_rx[...])[:, :1]
+    final = lax.rsqrt(total / width + 1e-06)
+    out_ref[...] = (home[...] * final * out_gain_ref[c]).astype(BF16)
+
+    for d in range(2):
+        for s in range(slots):
+            ag(s, d, rx.at[s, d, c]).wait_send()
+            pag(s, d, c).wait_send()
+            back(s, d).wait_send()
+        for i in range(turn):
+            agw(i, d, wrx.at[i, d, c]).wait_send()
+            pagw(i, d, c).wait_send()
+    for s in range(slots):
+        partner(s).wait_send()
+    for copy in home_copies:
+        copy(c).wait_send()
+    home_copy.wait_send()
+    sq_copy.wait_send()
+
+
+def ring_local(
+    n,
+    tokens,
+    expert_ids,
+    gate_weights,
+    norm_gain,
+    expert_gate,
+    expert_up,
+    expert_down,
+    shared_gate,
+    shared_up,
+    shared_down,
+    out_gain,
+):
+    rows, width = tokens.shape
+    ff = expert_gate.shape[2]
+    sh = shared_gate.shape[1]
+    cols = width // 2
+    slots, turn, half = n - 1, n // 2, rows // 2
+    experts = 2 * n * expert_gate.shape[0]
+    dma = pltpu.SemaphoreType.DMA
+    vmem = pl.BlockSpec(memory_space=pltpu.VMEM)
+    hbm = pl.BlockSpec(memory_space=pl.ANY)
+    return pl.pallas_call(
+        functools.partial(ring_kernel, n),
+        out_shape=jax.ShapeDtypeStruct((2 * rows, cols), BF16),
+        in_specs=[vmem] * 5 + [hbm] * 6,
+        out_specs=vmem,
+        scratch_shapes=[
+            pltpu.VMEM((2, rows, width), BF16),
+            pltpu.VMEM((2, experts, rows), F32),
+            pltpu.VMEM((slots, 2, 2, half, width), BF16),
+            pltpu.VMEM((turn, 2, 2, experts, rows), F32),
+            pltpu.VMEM((width, ff), BF16),
+            pltpu.VMEM((width, ff), BF16),
+            pltpu.VMEM((ff, cols), BF16),
+            pltpu.VMEM((ff, cols), BF16),
+            pltpu.VMEM((width, sh), BF16),
+            pltpu.VMEM((width, sh), BF16),
+            pltpu.VMEM((sh, cols), BF16),
+            pltpu.VMEM((sh, cols), BF16),
+            pltpu.VMEM((slots, 2 * rows, cols), F32),
+            pltpu.VMEM((slots, 2 * rows, cols), BF16),
+            pltpu.VMEM((slots, 2 * rows, cols), BF16),
+            pltpu.VMEM((2 * rows, cols), F32),
+            pltpu.VMEM((2 * rows, cols), F32),
+            pltpu.VMEM((2 * rows, cols), F32),
+            pltpu.VMEM((slots, 2, rows, cols), BF16),
+            pltpu.VMEM((slots, 2, rows, cols), BF16),
+            pltpu.VMEM((2 * rows, 128), F32),
+            pltpu.VMEM((2 * rows, 128), F32),
+            dma((8,)),
+            dma((slots, 2)),
+            dma((slots, 2)),
+            dma((turn, 2)),
+            dma((turn, 2)),
+            dma((slots, 2)),
+            dma((slots, 2)),
+            dma((turn, 2)),
+            dma((turn, 2)),
+            dma((2,)),
+            dma((2,)),
+            dma((slots,)),
+            dma((slots,)),
+            dma((1,)),
+            dma((1,)),
+            dma((slots, 2)),
+            dma((slots, 2)),
+            dma((1,)),
+            dma((1,)),
+        ],
+        compiler_params=pltpu.CompilerParams(
+            collective_id=0, has_side_effects=True, vmem_limit_bytes=60 * 1024 * 1024
+        ),
+    )(
+        expert_ids,
+        gate_weights,
+        tokens,
+        norm_gain.reshape(1, width),
+        out_gain.reshape(2, 1, cols),
+        expert_gate,
+        expert_up,
+        expert_down,
+        shared_gate,
+        shared_up,
+        shared_down,
+    )
+
 
 TOPK = 4
 
@@ -89,4 +475,17 @@
         P(),
     )
     out_specs = P(("grp", "ep"), "tp")
-    return jax.shard_map(local, mesh=mesh, in_specs=in_specs, out_specs=out_specs, check_vma=False)
+    n, tp = mesh.shape["ep"], mesh.shape["tp"]
+
+    def run(*args):
+        tokens, expert_gate = args[0], args[4]
+        rows = tokens.shape[0] // mesh.size
+        experts = expert_gate.shape[0]
+        dense = experts == n * tp and experts <= 8 * args[1].shape[1]
+        dense = dense and tp == 2 and n % 2 == 0 and n >= 4 and rows == 128
+        body = functools.partial(ring_local, n) if dense else local
+        return jax.shard_map(
+            body, mesh=mesh, in_specs=in_specs, out_specs=out_specs, check_vma=False
+        )(*args)
+
+    return run

time: 221 us -> 97 us (0.44)
  the two profiles are of different devices: /device:TPU:21 before, /device:TPU:1 now
where the time goes in v1:
time: 97 us; the launch traced here: 96.8 us
  Pallas kernels  92.1 us (95%)
  local copies, waits for them, and re-layouts  4.69 us (5%)
    pallas_call x1, Pallas kernels, ring_local(): pl.pallas_call(functools.partial(ring_kernel, n), out_shape=jax.ShapeDtyp...  92.1 us
    unnamed x3, local copies, waits for them, and re-layouts  4.69 us

profile of v1, /device:TPU:1, one launch (start us, length us, event | category | flops | bytes accessed | tf_op | source)
XLA Modules:
  0.0 96.8 jit_solution(9963133833059240905)
XLA Ops:
  0.0 1.4 %copy.12.ids_ref = s32[128,4]{1,0:T(8,128)} copy(s32[128,4]{0,1:T(4,128)} %param.12) | data formatting | bytes 4096 | tf_op args[1]
  1.4 1.4 %copy.13.gates_ref = f32[128,4]{1,0:T(8,128)} copy(f32[128,4]{0,1:T(4,128)} %param.13) | data formatting | bytes 4096 | tf_op args[2]
  2.8 92.1 %shard_map.109 = bf16[256,1024]{1,0:T(8,128)(2,1)} custom-call(s32[128,4]{1,0:T(8,128)} %copy.12.ids_ref, f32[128,4]{1,0:T(8,128)} %copy.13.gates_ref, bf16[128,2048]{1,0:T(8,128)(2,1)} %tok_ref.1, f32[1,2048]{1,0:T(1,128)} %bitcast.2, f32[2,1,1024]{2,1,0:T(1,128)} %bitcast.3, bf16[1,2048,512]{2,1,0:T(8,128)(2,1)} %eg_hbm.1, bf16[1,2048,512]{2,1,0:T(8,128)(2,1)} %eu_hbm.1, ...), custom_call_target="tpu_custom_call" | custom-call | tf_op jit(solution)/shard_map/pallas_call | solution.py:326
  95.0 1.9 %copy.15 = bf16[256,1024]{1,0:T(8,128)(2,1)} copy(bf16[256,1024]{1,0:T(8,128)(2,1)} %shard_map.109) | data formatting | bytes 1048576

commit v2 on v1

--- a/solution.py
+++ b/solution.py
@@ -8,6 +8,7 @@
 from jax.sharding import PartitionSpec as P
 
 MESH = pl.DeviceIdType.MESH
+PARTS = 2
 F32 = jnp.float32
 BF16 = jnp.bfloat16
 
@@ -18,7 +19,6 @@
     gates_ref,
     tok_ref,
     gain_ref,
-    out_gain_ref,
     eg_hbm,
     eu_hbm,
     ed_hbm,
@@ -26,6 +26,7 @@
     su_hbm,
     sd_hbm,
     out_ref,
+    sq_ref,
     own_x,
     own_w,
     rx,
@@ -68,11 +69,12 @@
     sq_ssem,
     sq_rsem,
 ):
-    slots = n - 1
+    per = 2 * PARTS
+    slots = (n - 1) * PARTS
     rows, width = tok_ref.shape
-    half = rows // 2
+    chunk = rows // per
     cols = width // 2
-    topk = ids_ref.shape[1]
+    topk = ids_ref.shape[0]
     experts = own_w.shape[1]
     turn = n // 2
     ep = lax.axis_index("ep")
@@ -112,11 +114,11 @@
     values = tok_ref[...].astype(F32)
     scale = lax.rsqrt(jnp.mean(values * values, axis=1, keepdims=True) + 1e-06)
     own_x[c] = (values * scale * gain_ref[...]).astype(BF16)
-    lane = lax.broadcasted_iota(jnp.int32, (rows, 128), 1)
-    dense = jnp.zeros((rows, 128), F32)
+    expert = lax.broadcasted_iota(jnp.int32, (experts, rows), 0)
+    dense = jnp.zeros((experts, rows), F32)
     for k in range(topk):
-        dense += jnp.where(ids_ref[:, k : k + 1] == lane, gates_ref[:, k : k + 1], 0.0)
-    own_w[c] = dense.T[:experts]
+        dense += jnp.where(ids_ref[k : k + 1, :] == expert, gates_ref[k : k + 1, :], 0.0)
+    own_w[c] = dense
 
     pl.semaphore_wait(barrier, 3)
 
@@ -146,20 +148,24 @@
             wrx.at[i, d, core], wrx.at[i, d, core], pw_ssem.at[i, d], pw_rsem.at[i, d], ep, oc
         )
 
-    def own_half(h):
-        return own_x.at[c, pl.ds(h * half, half)]
+    def place(s, d):
+        return (s + d * PARTS) % per
+
+    def own_chunk(s, d):
+        return own_x.at[c, pl.ds(place(s, d) * chunk, chunk)]
 
     for d in range(2):
         agw(0, d, own_w.at[c]).start()
-        ag(0, d, own_half(d)).start()
+        ag(0, d, own_chunk(0, d)).start()
     home_copies = (
         lambda core: remote(own_x.at[core], own_x.at[core], ox_ssem.at[0], ox_rsem.at[0], ep, oc),
         lambda core: remote(own_w.at[core], own_w.at[core], ox_ssem.at[1], ox_rsem.at[1], ep, oc),
     )
     for copy in home_copies:
         copy(c).start()
-    for d in range(2):
-        ag(1, d, own_half(1 - d)).start()
+    for s in range(1, per):
+        for d in range(2):
+            ag(s, d, own_chunk(s, d)).start()
 
     def silu_mul(g, u):
         return (g / (1.0 + jnp.exp(-g)) * u).astype(BF16)
@@ -192,22 +198,22 @@
         return remote(psend.at[s], prx.at[s], p_ssem.at[s], p_rsem.at[s], ep, oc)
 
     def step(s, _):
-        i = s // 2
-        even = s % 2 == 0
+        i = s // per
+        first = s % per == 0
         for d in range(2):
             ag(s, d, rx.at[s, d, c]).wait_recv()
 
-            @pl.when(s + 2 < slots)
+            @pl.when(s + per < slots)
             def _():
-                ag(s + 2, d, rx.at[s, d, c]).start()
+                ag(s + per, d, rx.at[s, d, c]).start()
 
             pag(s, d, c).start()
 
-            @pl.when(even)
+            @pl.when(first)
             def _():
                 agw(i, d, wrx.at[i, d, c]).wait_recv()
 
-                @pl.when(s + 2 < slots)
+                @pl.when(s + per < slots)
                 def _():
                     agw(i + 1, d, wrx.at[i, d, c]).start()
 
@@ -216,7 +222,7 @@
         for d in range(2):
             pag(s, d, oc).wait_recv()
 
-            @pl.when(even)
+            @pl.when(first)
             def _():
                 pagw(i, d, oc).wait_recv()
 
@@ -224,15 +230,15 @@
             [
                 column(
                     wrx[i, d, k, pl.ds(mine, 1), :],
-                    (s % 2) * half if d == 0 else (1 - s % 2) * half,
-                    half,
+                    place(s, d) * chunk,
+                    chunk,
                 )
                 for d in range(2)
                 for k in range(2)
             ],
             axis=0,
         )
-        xs = rx[s].reshape(2 * rows, width)
+        xs = rx[s].reshape(4 * chunk, width)
         hidden = silu_mul(dot(xs, wg[...]), dot(xs, wu[...]))
         psend[s] = (dot(hidden, wd_other[...]) * weight).astype(BF16)
         kept[s] = dot(hidden, wd_mine[...]) * weight
@@ -247,42 +253,41 @@
     def give(s, further):
         partner(s).wait_recv()
         for d in range(2):
-            part = pl.ds(d * rows, rows)
+            part = pl.ds(d * 2 * chunk, 2 * chunk)
             total = kept[s, part, :] + prx[s, part, :].astype(F32)
             if further:
-                back(s + 2, d).wait_recv()
-                total += rs_rx[s + 2, d].astype(F32)
+                back(s + per, d).wait_recv()
+                total += rs_rx[s + per, d].astype(F32)
             rs_send[s, d] = total.astype(BF16)
             back(s, d).start()
 
-    lax.fori_loop(0, slots - 1, step, 0)
-    give(slots - 2, False)
-    lax.fori_loop(slots - 1, slots, step, 0)
-    give(slots - 1, False)
-    for s in [t for k in range(slots - 4, -1, -2) for t in (k, k + 1)] + [0]:
+    for s in range(slots - per, slots):
+        lax.fori_loop(s if s > slots - per else 0, s + 1, step, 0)
+        give(s, False)
+    home_copy.wait_recv()
+    home[...] += home_rx[...]
+    order = [s for k in range(slots - 2 * per, -1, -per) for s in range(k, k + per)]
+    for s in order + list(range(slots % per)):
         give(s, True)
 
-    home_copy.wait_recv()
-    mixed = []
-    for s in range(2):
+    for s in [*range(PARTS, per), *range(PARTS)]:
         for d in range(2):
             back(s, d).wait_recv()
-    for k in range(2):
-        for h in range(2):
-            part = pl.ds(k * rows + h * half, half)
-            got = pl.ds(k * half, half)
-            total = home[part, :] + home_rx[part, :]
-            total += rs_rx[h, 0, got, :].astype(F32) + rs_rx[1 - h, 1, got, :].astype(F32)
-            rounded = total.astype(BF16).astype(F32)
-            home[part, :] = rounded
-            sq = jnp.sum(rounded * rounded, axis=1, keepdims=True)
-            sq_send[part, :] = jnp.broadcast_to(sq, (half, 128))
+            for k in range(2):
+                part = pl.ds(k * rows + place(s, d) * chunk, chunk)
+                total = home[part, :] + rs_rx[s, d, pl.ds(k * chunk, chunk), :].astype(F32)
+                if s >= PARTS:
+                    home[part, :] = total
+                else:
+                    mixed = total.astype(BF16)
+                    out_ref[part, :] = mixed
+                    mixed = mixed.astype(F32)
+                    sq = jnp.sum(mixed * mixed, axis=1, keepdims=True)
+                    sq_send[part, :] = jnp.broadcast_to(sq, (chunk, 128))
     sq_copy = remote(sq_send, sq_rx, sq_ssem.at[0], sq_rsem.at[0], ep, oc)
     sq_copy.start()
     sq_copy.wait_recv()
-    total = (sq_send[...] + sq_rx[...])[:, :1]
-    final = lax.rsqrt(total / width + 1e-06)
-    out_ref[...] = (home[...] * final * out_gain_ref[c]).astype(BF16)
+    sq_ref[...] = sq_send[...] + sq_rx[...]
 
     for d in range(2):
         for s in range(slots):
@@ -318,20 +323,24 @@
     ff = expert_gate.shape[2]
     sh = shared_gate.shape[1]
     cols = width // 2
-    slots, turn, half = n - 1, n // 2, rows // 2
+    slots, turn = (n - 1) * PARTS, n // 2
+    chunk = rows // (2 * PARTS)
     experts = 2 * n * expert_gate.shape[0]
     dma = pltpu.SemaphoreType.DMA
     vmem = pl.BlockSpec(memory_space=pltpu.VMEM)
     hbm = pl.BlockSpec(memory_space=pl.ANY)
-    return pl.pallas_call(
+    mixed, squares = pl.pallas_call(
         functools.partial(ring_kernel, n),
-        out_shape=jax.ShapeDtypeStruct((2 * rows, cols), BF16),
-        in_specs=[vmem] * 5 + [hbm] * 6,
-        out_specs=vmem,
+        out_shape=(
+            jax.ShapeDtypeStruct((2 * rows, cols), BF16),
+            jax.ShapeDtypeStruct((2 * rows, 128), F32),
+        ),
+        in_specs=[vmem] * 4 + [hbm] * 6,
+        out_specs=(vmem, vmem),
         scratch_shapes=[
             pltpu.VMEM((2, rows, width), BF16),
             pltpu.VMEM((2, experts, rows), F32),
-            pltpu.VMEM((slots, 2, 2, half, width), BF16),
+            pltpu.VMEM((slots, 2, 2, chunk, width), BF16),
             pltpu.VMEM((turn, 2, 2, experts, rows), F32),
             pltpu.VMEM((width, ff), BF16),
             pltpu.VMEM((width, ff), BF16),
@@ -341,14 +350,14 @@
             pltpu.VMEM((width, sh), BF16),
             pltpu.VMEM((sh, cols), BF16),
             pltpu.VMEM((sh, cols), BF16),
-            pltpu.VMEM((slots, 2 * rows, cols), F32),
-            pltpu.VMEM((slots, 2 * rows, cols), BF16),
-            pltpu.VMEM((slots, 2 * rows, cols), BF16),
+            pltpu.VMEM((slots, 4 * chunk, cols), F32),
+            pltpu.VMEM((slots, 4 * chunk, cols), BF16),
+            pltpu.VMEM((slots, 4 * chunk, cols), BF16),
             pltpu.VMEM((2 * rows, cols), F32),
             pltpu.VMEM((2 * rows, cols), F32),
             pltpu.VMEM((2 * rows, cols), F32),
-            pltpu.VMEM((slots, 2, rows, cols), BF16),
-            pltpu.VMEM((slots, 2, rows, cols), BF16),
+            pltpu.VMEM((slots, 2, 2 * chunk, cols), BF16),
+            pltpu.VMEM((slots, 2, 2 * chunk, cols), BF16),
             pltpu.VMEM((2 * rows, 128), F32),
             pltpu.VMEM((2 * rows, 128), F32),
             dma((8,)),
@@ -375,11 +384,10 @@
             collective_id=0, has_side_effects=True, vmem_limit_bytes=60 * 1024 * 1024
         ),
     )(
-        expert_ids,
-        gate_weights,
+        expert_ids.T,
+        gate_weights.T,
         tokens,
         norm_gain.reshape(1, width),
-        out_gain.reshape(2, 1, cols),
         expert_gate,
         expert_up,
         expert_down,
@@ -387,6 +395,9 @@
         shared_up,
         shared_down,
     )
+    scale = lax.rsqrt(squares[:, :1] / width + 1e-06)
+    gain = lax.dynamic_slice(out_gain, (lax.axis_index("tp") * cols,), (cols,))
+    return (mixed.astype(F32) * scale * gain).astype(BF16)
 
 
 TOPK = 4

time: 97 us -> 94.5 us (0.974)
  local copies, waits for them, and re-layouts: 4.69 us -> 0.01 us
  other arithmetic: 0 us -> 3.05 us
    unnamed x3 -> x0, local copies, waits for them, and re-layouts: 4.69 us -> none
    convert_element_type x0 -> x1, other arithmetic: none -> 2.02 us  [ring_local(): return (mixed.astype(F32) * scale * gain).astype(BF16)]
    rsqrt x0 -> x1, other arithmetic: none -> 1.02 us  [ring_local(): scale = lax.rsqrt(squares[:, :1] / width + 1e-06)]
where the time goes in v2:
time: 94.5 us; the launch traced here: 94.3 us
  Pallas kernels  91.2 us (97%)
  other arithmetic  3.05 us (3%)
    pallas_call x1, Pallas kernels, ring_local(): pl.pallas_call(functools.partial(ring_kernel, n), out_shape=(jax.ShapeDty...  91.2 us
    convert_element_type x1, other arithmetic, ring_local(): return (mixed.astype(F32) * scale * gain).astype(BF16)  2.02 us

profile of v2, /device:TPU:1, one launch (start us, length us, event | category | flops | bytes accessed | tf_op | source)
XLA Modules:
  0.0 94.3 jit_solution(18179395755831769136)
XLA Ops:
  0.0 0.0 dynamic-slice-start
  0.0 91.2 %shard_map.109 = (bf16[256,1024]{1,0:T(8,128)(2,1)}, f32[256,128]{1,0:T(8,128)}) custom-call(s32[4,128]{1,0:T(4,128)} %bitcast.4, f32[4,128]{1,0:T(4,128)} %bitcast.5, bf16[128,2048]{1,0:T(8,128)(2,1)} %tok_ref.1, f32[1,2048]{1,0:T(1,128)} %bitcast.3, bf16[1,2048,512]{2,1,0:T(8,128)(2,1)} %eg_hbm.1, bf16[1,2048,512]{2,1,0:T(8,128)(2,1)} %eu_hbm.1, ...), custom_call_target="tpu_custom_call" | custom-call | tf_op jit(solution)/shard_map/pallas_call | solution.py:332
  91.2 1.0 %rsqrt_reduce_fusion = f32[256]{0:T(256)S(1)} fusion(f32[256,128]{1,0:T(8,128)} %get-tuple-element.8), kind=kLoop, calls=%fused_computation.1 | loop fusion | flops 512 | bytes 2048 | tf_op jit(solution)/shard_map/rsqrt | solution.py:398
  92.2 0.0 dynamic-slice-done
  92.2 2.0 %multiply_convert_fusion = bf16[256,1024]{1,0:T(8,128)(2,1)} fusion(bf16[256,1024]{1,0:T(8,128)(2,1)} %get-tuple-element.7, f32[1024]{0:T(1024)S(1)} %dynamic-slice-done, f32[256]{0:T(256)S(1)} %rsqrt_reduce_fusion), kind=kLoop, calls=%fused_computation | loop fusion | flops 1048576 | bytes 1053696 | tf_op jit(solution)/shard_map/convert_element_type | solution.py:400
Async XLA Ops:
  0.0 92.2 %dynamic-slice-start = ((f32[2048]{0:T(1024)}, s32[]{:T(128)}), f32[1024]{0:T(1024)S(1)}, s32[]{:S(2)}) async-start(f32[2048]{0:T(1024)} %param.21, s32[]{:T(128)} %select_n.3), calls=%async_computation | async-start | bytes 8704 | tf_op jit(solution)/shard_map/dynamic_slice | solution.py:399

commit v3 on v2

--- a/solution.py
+++ b/solution.py
@@ -17,8 +17,9 @@
     n,
     ids_ref,
     gates_ref,
-    tok_ref,
+    tok_hbm,
     gain_ref,
+    out_gain_ref,
     eg_hbm,
     eu_hbm,
     ed_hbm,
@@ -26,7 +27,7 @@
     su_hbm,
     sd_hbm,
     out_ref,
-    sq_ref,
+    tok,
     own_x,
     own_w,
     rx,
@@ -49,6 +50,7 @@
     rs_rx,
     sq_send,
     sq_rx,
+    tok_sem,
     load_sem,
     ag_ssem,
     ag_rsem,
@@ -71,7 +73,7 @@
 ):
     per = 2 * PARTS
     slots = (n - 1) * PARTS
-    rows, width = tok_ref.shape
+    rows, width = tok.shape
     chunk = rows // per
     cols = width // 2
     topk = ids_ref.shape[0]
@@ -95,6 +97,12 @@
     for e in toward:
         pl.semaphore_signal(barrier, inc=1, device_id={"ep": e, "tp": c}, device_id_type=MESH)
     pl.semaphore_signal(barrier, inc=1, device_id={"ep": ep, "tp": oc}, device_id_type=MESH)
+
+    tok_loads = []
+    for j, k in enumerate([k for s in range(PARTS) for k in (s, s + PARTS)]):
+        part = pl.ds(k * chunk, chunk)
+        tok_loads.append(pltpu.make_async_copy(tok_hbm.at[part], tok.at[part], tok_sem.at[j]))
+        tok_loads[-1].start()
 
     lo, hi = pl.ds(pl.multiple_of(c * cols, cols), cols), pl.ds(pl.multiple_of(oc * cols, cols), cols)
     loads = [
@@ -111,16 +119,11 @@
     for load in loads:
         load.start()
 
-    values = tok_ref[...].astype(F32)
-    scale = lax.rsqrt(jnp.mean(values * values, axis=1, keepdims=True) + 1e-06)
-    own_x[c] = (values * scale * gain_ref[...]).astype(BF16)
     expert = lax.broadcasted_iota(jnp.int32, (experts, rows), 0)
     dense = jnp.zeros((experts, rows), F32)
     for k in range(topk):
         dense += jnp.where(ids_ref[k : k + 1, :] == expert, gates_ref[k : k + 1, :], 0.0)
     own_w[c] = dense
-
-    pl.semaphore_wait(barrier, 3)
 
     def remote(src, dst, ssem, rsem, e, core):
         return pltpu.make_async_remote_copy(
@@ -154,18 +157,31 @@
     def own_chunk(s, d):
         return own_x.at[c, pl.ds(place(s, d) * chunk, chunk)]
 
-    for d in range(2):
-        agw(0, d, own_w.at[c]).start()
-        ag(0, d, own_chunk(0, d)).start()
+    def normalise(k):
+        part = pl.ds(k * chunk, chunk)
+        values = tok[part, :].astype(F32)
+        scale = lax.rsqrt(jnp.mean(values * values, axis=1, keepdims=True) + 1e-06)
+        own_x[c, part, :] = (values * scale * gain_ref[...]).astype(BF16)
+
+    for s in range(PARTS):
+        for d in range(2):
+            tok_loads[2 * s + d].wait()
+            normalise(s + d * PARTS)
+        if s == 0:
+            pl.semaphore_wait(barrier, 3)
+            for d in range(2):
+                agw(0, d, own_w.at[c]).start()
+        for d in range(2):
+            ag(s, d, own_chunk(s, d)).start()
+    for s in range(PARTS, per):
+        for d in range(2):
+            ag(s, d, own_chunk(s, d)).start()
     home_copies = (
         lambda core: remote(own_x.at[core], own_x.at[core], ox_ssem.at[0], ox_rsem.at[0], ep, oc),
         lambda core: remote(own_w.at[core], own_w.at[core], ox_ssem.at[1], ox_rsem.at[1], ep, oc),
     )
     for copy in home_copies:
         copy(c).start()
-    for s in range(1, per):
-        for d in range(2):
-            ag(s, d, own_chunk(s, d)).start()
 
     def silu_mul(g, u):
         return (g / (1.0 + jnp.exp(-g)) * u).astype(BF16)
@@ -270,24 +286,37 @@
     for s in order + list(range(slots % per)):
         give(s, True)
 
+    def squares(s):
+        return remote(sq_send.at[s], sq_rx.at[s], sq_ssem.at[s], sq_rsem.at[s], ep, oc)
+
+    def home_rows(s, d, k):
+        return pl.ds(k * rows + place(s, d) * chunk, chunk)
+
     for s in [*range(PARTS, per), *range(PARTS)]:
         for d in range(2):
             back(s, d).wait_recv()
             for k in range(2):
-                part = pl.ds(k * rows + place(s, d) * chunk, chunk)
+                part = home_rows(s, d, k)
                 total = home[part, :] + rs_rx[s, d, pl.ds(k * chunk, chunk), :].astype(F32)
-                if s >= PARTS:
-                    home[part, :] = total
-                else:
-                    mixed = total.astype(BF16)
-                    out_ref[part, :] = mixed
-                    mixed = mixed.astype(F32)
-                    sq = jnp.sum(mixed * mixed, axis=1, keepdims=True)
-                    sq_send[part, :] = jnp.broadcast_to(sq, (chunk, 128))
-    sq_copy = remote(sq_send, sq_rx, sq_ssem.at[0], sq_rsem.at[0], ep, oc)
-    sq_copy.start()
-    sq_copy.wait_recv()
-    sq_ref[...] = sq_send[...] + sq_rx[...]
+                if s < PARTS:
+                    total = total.astype(BF16).astype(F32)
+                    sq = jnp.sum(total * total, axis=1, keepdims=True)
+                    sq_send[s, pl.ds((2 * d + k) * chunk, chunk), :] = jnp.broadcast_to(
+                        sq, (chunk, 128)
+                    )
+                home[part, :] = total
+        if s < PARTS:
+            squares(s).start()
+    for s in range(PARTS):
+        squares(s).wait_recv()
+        final = lax.rsqrt((sq_send[s] + sq_rx[s])[:, :1] / width + 1e-06)
+        for d in range(2):
+            for k in range(2):
+                part = home_rows(s, d, k)
+                at_k = (2 * d + k) * chunk
+                out_ref[part, :] = (
+                    home[part, :] * final[at_k : at_k + chunk] * out_gain_ref[c]
+                ).astype(BF16)
 
     for d in range(2):
         for s in range(slots):
@@ -302,7 +331,8 @@
     for copy in home_copies:
         copy(c).wait_send()
     home_copy.wait_send()
-    sq_copy.wait_send()
+    for s in range(PARTS):
+        squares(s).wait_send()
 
 
 def ring_local(
@@ -329,15 +359,13 @@
     dma = pltpu.SemaphoreType.DMA
     vmem = pl.BlockSpec(memory_space=pltpu.VMEM)
     hbm = pl.BlockSpec(memory_space=pl.ANY)
-    mixed, squares = pl.pallas_call(
+    return pl.pallas_call(
         functools.partial(ring_kernel, n),
-        out_shape=(
-            jax.ShapeDtypeStruct((2 * rows, cols), BF16),
-            jax.ShapeDtypeStruct((2 * rows, 128), F32),
-        ),
-        in_specs=[vmem] * 4 + [hbm] * 6,
-        out_specs=(vmem, vmem),
+        out_shape=pltpu.VMEM((2 * rows, cols), BF16),
+        in_specs=[vmem] * 2 + [hbm] + [vmem] * 2 + [hbm] * 6,
+        out_specs=vmem,
         scratch_shapes=[
+            pltpu.VMEM((rows, width), BF16),
             pltpu.VMEM((2, rows, width), BF16),
             pltpu.VMEM((2, experts, rows), F32),
             pltpu.VMEM((slots, 2, 2, chunk, width), BF16),
@@ -358,8 +386,9 @@
             pltpu.VMEM((2 * rows, cols), F32),
             pltpu.VMEM((slots, 2, 2 * chunk, cols), BF16),
             pltpu.VMEM((slots, 2, 2 * chunk, cols), BF16),
-            pltpu.VMEM((2 * rows, 128), F32),
-            pltpu.VMEM((2 * rows, 128), F32),
+            pltpu.VMEM((PARTS, 4 * chunk, 128), F32),
+            pltpu.VMEM((PARTS, 4 * chunk, 128), F32),
+            dma((2 * PARTS,)),
             dma((8,)),
             dma((slots, 2)),
             dma((slots, 2)),
@@ -377,8 +406,8 @@
             dma((1,)),
             dma((slots, 2)),
             dma((slots, 2)),
-            dma((1,)),
-            dma((1,)),
+            dma((PARTS,)),
+            dma((PARTS,)),
         ],
         compiler_params=pltpu.CompilerParams(
             collective_id=0, has_side_effects=True, vmem_limit_bytes=60 * 1024 * 1024
@@ -388,6 +417,7 @@
         gate_weights.T,
         tokens,
         norm_gain.reshape(1, width),
+        out_gain.reshape(2, 1, cols),
         expert_gate,
         expert_up,
         expert_down,
@@ -395,9 +425,6 @@
         shared_up,
         shared_down,
     )
-    scale = lax.rsqrt(squares[:, :1] / width + 1e-06)
-    gain = lax.dynamic_slice(out_gain, (lax.axis_index("tp") * cols,), (cols,))
-    return (mixed.astype(F32) * scale * gain).astype(BF16)
 
 
 TOPK = 4

time: 94.5 us -> 92.8 us (0.982)
  other arithmetic: 3.05 us -> 0 us
    convert_element_type x1 -> x0, other arithmetic: 2.02 us -> none  [ring_local(): return (mixed.astype(F32) * scale * gain).astype(BF16)]
    rsqrt x1 -> x0, other arithmetic: 1.02 us -> none  [ring_local(): scale = lax.rsqrt(squares[:, :1] / width + 1e-06)]
where the time goes in v3:
time: 92.8 us; the launch traced here: 92.6 us
  Pallas kernels  91.8 us (99%)
    pallas_call x1, Pallas kernels, ring_local(): pl.pallas_call(functools.partial(ring_kernel, n), out_shape=pltpu.VMEM((2...  91.8 us

profile of v3, /device:TPU:1, one launch (start us, length us, event | category | flops | bytes accessed | tf_op | source)
XLA Modules:
  0.0 92.6 jit_solution(9040725050177645400)
XLA Ops:
  0.0 91.8 %shard_map.109 = bf16[256,1024]{1,0:T(8,128)(2,1)S(1)} custom-call(s32[4,128]{1,0:T(4,128)} %bitcast.6, f32[4,128]{1,0:T(4,128)} %bitcast.7, bf16[128,2048]{1,0:T(8,128)(2,1)} %tok_hbm.1, f32[1,2048]{1,0:T(1,128)} %bitcast.4, f32[2,1,1024]{2,1,0:T(1,128)} %bitcast.5, bf16[1,2048,512]{2,1,0:T(8,128)(2,1)} %eg_hbm.1, bf16[1,2048,512]{2,1,0:T(8,128)(2,1)} %eu_hbm.1, ...), custom_call_target="tpu_custom_call" | custom-call | tf_op jit(solution)/shard_map/pallas_call | solution.py:362
  91.8 0.8 copy.13

commit v4 on v3

--- a/solution.py
+++ b/solution.py
@@ -183,6 +183,30 @@
     for copy in home_copies:
         copy(c).start()
 
+    def relay(s):
+        i = s // per
+        first = s % per == 0
+        for d in range(2):
+            ag(s, d, rx.at[s, d, c]).wait_recv()
+
+            @pl.when(s + per < slots)
+            def _():
+                ag(s + per, d, rx.at[s, d, c]).start()
+
+            pag(s, d, c).start()
+
+            @pl.when(first)
+            def _():
+                agw(i, d, wrx.at[i, d, c]).wait_recv()
+
+                @pl.when(s + per < slots)
+                def _():
+                    agw(i + 1, d, wrx.at[i, d, c]).start()
+
+                pagw(i, d, c).start()
+
+    relay(0)
+
     def silu_mul(g, u):
         return (g / (1.0 + jnp.exp(-g)) * u).astype(BF16)
 
@@ -213,28 +237,9 @@
     def partner(s):
         return remote(psend.at[s], prx.at[s], p_ssem.at[s], p_rsem.at[s], ep, oc)
 
-    def step(s, _):
+    def work(s):
         i = s // per
         first = s % per == 0
-        for d in range(2):
-            ag(s, d, rx.at[s, d, c]).wait_recv()
-
-            @pl.when(s + per < slots)
-            def _():
-                ag(s + per, d, rx.at[s, d, c]).start()
-
-            pag(s, d, c).start()
-
-            @pl.when(first)
-            def _():
-                agw(i, d, wrx.at[i, d, c]).wait_recv()
-
-                @pl.when(s + per < slots)
-                def _():
-                    agw(i + 1, d, wrx.at[i, d, c]).start()
-
-                pagw(i, d, c).start()
-
         for d in range(2):
             pag(s, d, oc).wait_recv()
 
@@ -259,7 +264,6 @@
         psend[s] = (dot(hidden, wd_other[...]) * weight).astype(BF16)
         kept[s] = dot(hidden, wd_mine[...]) * weight
         partner(s).start()
-        return 0
 
     def back(s, d):
         return remote(
@@ -277,9 +281,20 @@
             rs_send[s, d] = total.astype(BF16)
             back(s, d).start()
 
+    def step(s, _):
+        relay(s + 1)
+        work(s)
+        return 0
+
+    lax.fori_loop(0, slots - per, step, 0)
     for s in range(slots - per, slots):
-        lax.fori_loop(s if s > slots - per else 0, s + 1, step, 0)
-        give(s, False)
+        if s + 1 < slots:
+            lax.fori_loop(s, s + 1, step, 0)
+        else:
+            work(s)
+        if s > slots - per:
+            give(s - 1, False)
+    give(slots - 1, False)
     home_copy.wait_recv()
     home[...] += home_rx[...]
     order = [s for k in range(slots - 2 * per, -1, -per) for s in range(k, k + per)]

time: 92.8 us -> 92.5 us (level)
  no operation moved by 1% of the time
where the time goes in v4:
time: 92.5 us; the launch traced here: 92.3 us
  Pallas kernels  91.5 us (99%)
    pallas_call x1, Pallas kernels, ring_local(): pl.pallas_call(functools.partial(ring_kernel, n), out_shape=pltpu.VMEM((2...  91.5 us

profile of v4, /device:TPU:1, one launch (start us, length us, event | category | flops | bytes accessed | tf_op | source)
XLA Modules:
  0.0 92.3 jit_solution(4708971440888860594)
XLA Ops:
  0.0 91.5 %shard_map.109 = bf16[256,1024]{1,0:T(8,128)(2,1)S(1)} custom-call(s32[4,128]{1,0:T(4,128)} %bitcast.6, f32[4,128]{1,0:T(4,128)} %bitcast.7, bf16[128,2048]{1,0:T(8,128)(2,1)} %tok_hbm.1, f32[1,2048]{1,0:T(1,128)} %bitcast.4, f32[2,1,1024]{2,1,0:T(1,128)} %bitcast.5, bf16[1,2048,512]{2,1,0:T(8,128)(2,1)} %eg_hbm.1, bf16[1,2048,512]{2,1,0:T(8,128)(2,1)} %eu_hbm.1, ...), custom_call_target="tpu_custom_call" | custom-call | tf_op jit(solution)/shard_map/pallas_call | solution.py:377
  91.5 0.8 copy.13
